TPU v7x, 256 devices: a whole 4x4x8 slice. The times are simulated.
256 devices in a mesh: ep: 32 (over z, x), tp: 8 (over y, core).
Axes of the slice: x: 4, y: 4, z: 8, core: 2. Of those that a mesh axis runs over, the one named last changes fastest.
Arguments:
- queries: bfloat16 [32768, 2048], P('ep', 'tp'), may hold values from -6 to 6
- key_vectors: bfloat16 [32768, 2048], P('ep', 'tp'), may hold values from -6 to 6
- value_vectors: bfloat16 [32768, 4096], P('ep', 'tp'), may hold values from -6 to 6
- decay_logit: float32 [32768, 2048], P('ep', 'tp'), may hold values from -11 to 16
- head_gain: float32 [256], replicated, may hold values from 0.1 to 1.9
- routed_rows: bfloat16 [8192, 4096], P('ep'), may hold values from -6 to 6
- pre_gain: float32 [4096], replicated, may hold values from 0.1 to 1.9
- expert_pick: int32 [8192, 2], P('ep'), may hold values from 0 to 31, as said below
- route_weight: float32 [8192, 2], P('ep'), may hold values from 0.2 to 1
- gate_weight: bfloat16 [32, 4096, 2048], P('ep', None, 'tp'), may hold values from -0.09375 to 0.09375
- up_weight: bfloat16 [32, 4096, 2048], P('ep', None, 'tp'), may hold values from -0.09375 to 0.09375
- down_weight: bfloat16 [32, 2048, 4096], P('ep', 'tp'), may hold values from -0.125 to 0.125
- post_gain: float32 [4096], replicated, may hold values from 0.1 to 1.9
Outputs:
- mixed_heads: bfloat16 [32768, 4096], P('ep', 'tp')
- routed_out: bfloat16 [8192, 4096], P(('ep', 'tp'))
Inputs may be any that keep to these rules, and one draw needn't show every extreme that they name: `expert_pick`: each row names 2 different experts, both in the same one of 4 equal groups of consecutive expert numbers. In every aligned block of 32 rows no expert is named more than 4 times, and some expert exactly 4 times.
All inputs are finite; a program needn't handle non-finite values.
Results may differ from a plain program's by a relative error of at most 0.015.
Values may be sent and summed in bfloat16 or wider, within the bound.
A program may use at most 128 MiB of HBM per device.

v0:
```python
import jax
import jax.numpy as jnp
from jax import lax
from jax.sharding import Mesh
from jax.sharding import PartitionSpec as P

DK = 128
DV = 256
BLK = 64
EP = ("ep_0", "ep_1")
EP_TP = ("ep_0", "ep_1", "tp")


def neutral_like(x, identity):
    return jax.tree.map(
        lambda part, zero: jnp.zeros_like(part) + jnp.asarray(zero, part.dtype), x, identity
    )


def prefix_by_axis(x, axes, combine, identity):
    before = start = neutral_like(x, identity)
    running = x
    for axis in reversed(axes):
        length, index = (lax.axis_size(axis), lax.axis_index(axis))
        pieces = jax.tree.map(
            lambda part, kind: lax.all_gather(part.astype(kind), axis),
            running,
            (jnp.bfloat16, jnp.bfloat16),
        )
        inside, running = (start, start)
        for k in range(length):
            passed = k < index
            running = combine(
                running, jax.tree.map(lambda part, own: part[k].astype(own.dtype), pieces, x)
            )
            inside = jax.tree.map(lambda new, old: jnp.where(passed, new, old), running, inside)
        before = combine(inside, before)
    return before


def chain_join(earlier, later_part):
    decay_first, initial_memory_matrix = earlier
    decay_second, state_second = later_part
    return (
        decay_first * decay_second,
        initial_memory_matrix * decay_second[..., None] + state_second,
    )


def row_norm(values, gain):
    return values * lax.rsqrt(jnp.mean(values * values, axis=-1, keepdims=True) + 1e-06) * gain


def token_mixer(queries, key_vectors, value_vectors, decay_logit, head_gain):
    blocks = queries.shape[0] // BLK
    heads_here = queries.shape[1] // DK
    key_shape = (blocks, BLK, heads_here, DK)
    log_rate = jax.nn.log_sigmoid(decay_logit).reshape(key_shape) / 16.0
    cumulative = jnp.cumsum(log_rate, axis=1)
    ending = cumulative[:, -1]
    query_rows = queries.reshape(key_shape)
    key_rows = key_vectors.reshape(key_shape)
    value_rows = value_vectors.reshape(blocks, BLK, heads_here, DV)
    query_decay = (query_rows * jnp.exp(cumulative)).astype(jnp.bfloat16)
    key_decay = (key_rows * jnp.exp(-cumulative)).astype(jnp.bfloat16)
    key_to_end = (key_rows * jnp.exp(ending[:, None] - cumulative)).astype(jnp.bfloat16)
    update = jnp.einsum(
        "njhd,njhe->nhde", key_to_end, value_rows, preferred_element_type=jnp.float32
    )
    step_decay = jnp.exp(ending)

    def advance(carry, inputs):
        carry_state, carry_decay = carry
        block_update, block_decay = inputs
        next_carry = (
            carry_state * block_decay[..., None] + block_update,
            carry_decay * block_decay,
        )
        return (next_carry, (carry_state, carry_decay))

    start_carry = (jnp.zeros_like(update[0]), jnp.ones_like(step_decay[0]))
    (final_state, total_decay), (local_states, local_decay) = lax.scan(
        advance, start_carry, (update, step_decay)
    )
    incoming = prefix_by_axis(
        (total_decay, final_state),
        EP,
        chain_join,
        (jnp.ones_like(total_decay), jnp.zeros_like(final_state)),
    )
    causal_mask = jnp.tril(jnp.ones((BLK, BLK), dtype=bool))
    scores = jnp.einsum(
        "nihd,njhd->nhij", query_decay, key_decay, preferred_element_type=jnp.float32
    )
    weights = jnp.where(causal_mask, scores, 0.0).astype(jnp.bfloat16)
    inside = jnp.einsum("nhij,njhe->nihe", weights, value_rows, preferred_element_type=jnp.float32)
    states = (local_states + incoming[1][None] * local_decay[..., None]).astype(jnp.bfloat16)
    carried = jnp.einsum("nihd,nhde->nihe", query_decay, states, preferred_element_type=jnp.float32)
    outputs = row_norm(inside + carried, head_gain).astype(jnp.bfloat16)
    return outputs.reshape(queries.shape[0], heads_here * DV)


def routed_experts(
    routed_rows, pre_gain, expert_pick, route_weight, gate_weight, up_weight, down_weight, post_gain
):
    tp_count = lax.axis_size("tp")
    ep_count = lax.axis_size(EP)
    part_index = lax.axis_index("tp")
    ep_rows, model_width = routed_rows.shape
    part_rows = ep_rows // tp_count
    top_count = expert_pick.shape[1]
    experts = ep_count * gate_weight.shape[0]
    capacity = 2 * top_count * part_rows // experts
    normed = row_norm(routed_rows.astype(jnp.float32), pre_gain).astype(jnp.bfloat16)
    padded = jnp.concatenate([normed, jnp.zeros((1, model_width), jnp.bfloat16)], axis=0)
    picks = expert_pick.reshape(tp_count, part_rows * top_count)
    matches = (picks[:, :, None] == jnp.arange(experts, dtype=jnp.int32)[None, None, :]).astype(
        jnp.int32
    )
    slots = jnp.sum((jnp.cumsum(matches, axis=1) - 1) * matches, axis=2)
    targets = picks * capacity + slots
    sources = (
        jnp.arange(part_rows * top_count, dtype=jnp.int32)[None, :] // top_count
        + part_rows * jnp.arange(tp_count, dtype=jnp.int32)[:, None]
    )
    slice_offset_index = jnp.broadcast_to(
        jnp.arange(tp_count, dtype=jnp.int32)[:, None], targets.shape
    )
    table = (
        jnp.full((tp_count, experts * capacity), ep_rows, jnp.int32)
        .at[slice_offset_index, targets]
        .set(sources)
    )
    gate_local = gate_weight[0]
    up_local = up_weight[0]
    down_local = down_weight[0]
    own_table = lax.dynamic_slice_in_dim(table, part_index, 1, 0)
    outgoing = padded[own_table].reshape(1, ep_count, capacity, model_width)
    arrived = lax.all_gather(
        lax.all_to_all(outgoing, EP, split_axis=1, concat_axis=1, tiled=True),
        "tp",
        axis=0,
        tiled=True,
    )
    gate_act = jnp.einsum("pskd,df->pskf", arrived, gate_local, preferred_element_type=jnp.float32)
    up_act = jnp.einsum("pskd,df->pskf", arrived, up_local, preferred_element_type=jnp.float32)
    hidden = (jax.nn.silu(gate_act) * up_act).astype(jnp.bfloat16)
    summed = lax.psum_scatter(
        jnp.einsum("pskf,fd->pskd", hidden, down_local, preferred_element_type=jnp.float32).astype(
            jnp.bfloat16
        ),
        "tp",
        scatter_dimension=0,
        tiled=True,
    )
    returned = lax.all_to_all(summed, EP, split_axis=1, concat_axis=1, tiled=True)
    flattened = returned.reshape(experts * capacity, model_width)
    my_slots = lax.dynamic_slice_in_dim(targets, part_index, 1, 0).reshape(part_rows, top_count)
    my_weight = lax.dynamic_slice_in_dim(route_weight, part_index * part_rows, part_rows, 0)
    combined = jnp.sum(flattened[my_slots].astype(jnp.float32) * my_weight[:, :, None], axis=1)
    return row_norm(combined, post_gain).astype(jnp.bfloat16)


def on_device(
    queries,
    key_vectors,
    value_vectors,
    decay_logit,
    head_gain,
    routed_rows,
    pre_gain,
    expert_pick,
    route_weight,
    gate_weight,
    up_weight,
    down_weight,
    post_gain,
):
    mixed_heads = token_mixer(queries, key_vectors, value_vectors, decay_logit, head_gain)
    routed_out = routed_experts(
        routed_rows,
        pre_gain,
        expert_pick,
        route_weight,
        gate_weight,
        up_weight,
        down_weight,
        post_gain,
    )
    return (mixed_heads, routed_out)


def solution(mesh):
    torus = Mesh(mesh.devices.reshape(8, 4, mesh.shape["tp"]), ("ep_0", "ep_1", "tp"))
    placed = (
        P(EP, "tp"),
        P(EP, "tp"),
        P(EP, "tp"),
        P(EP, "tp"),
        P(),
        P(EP, None),
        P(),
        P(EP, None),
        P(EP, None),
        P(EP, None, "tp"),
        P(EP, None, "tp"),
        P(EP, "tp", None),
        P(),
    )
    return jax.shard_map(
        on_device,
        mesh=torus,
        in_specs=placed,
        out_specs=(P(EP, "tp"), P(EP_TP, None)),
        check_vma=False,
    )
```

profile of v0, /device:TPU:2, one launch (start us, length us, event | category | flops | bytes accessed | tf_op | source)
XLA Modules:
  0.0 290.8 jit_solution(14638093598080471657)
XLA Ops:
  8.1 0.9 copy.95
  9.9 1.3 fusion.73
  11.9 22.1 %scatter_fusion = s32[8,128]{1,0:T(8,128)S(1)} fusion(s32[8,128]{1,0:T(8,128)S(1)} %broadcast_in_dim.33, s32[512]{0:T(512)S(1)} %reshape.309, s32[512]{0:T(512)S(1)} %reshape.311), kind=kCustom, calls=%fused_computation.2 | custom fusion | bytes 10240 | tf_op jit(solution)/shard_map/scatter | solution.py:132
  34.0 2.1 fusion.1
  36.1 2.2 fusion.3
  38.4 1.5 concatenate.6
  39.9 4.1 %gather_fusion = bf16[128,4096]{1,0:T(8,128)(2,1)S(1)} fusion(bf16[257,4096]{1,0:T(8,128)(2,1)} %concatenate.6, s32[1024]{0:T(1024)S(1)} %pad_clamp_fusion.1), kind=kCustom, calls=%fused_computation | custom fusion | bytes 2097664 | tf_op jit(solution)/shard_map/gather | solution.py:138
  44.0 1.2 reshape.277
  45.2 39.7 %all_to_all.10 = bf16[1,32,4,4096]{3,2,0,1:T(4,128)(2,1)S(1)} all-to-all(bf16[1,32,4,4096]{3,2,0,1:T(4,128)(2,1)} %bitcast.178), channel_id=1, replica_groups=mesh['ep_0'=8,'ep_1'=4,'tp'=8] {'ep_0','ep_1'}, dimensions={1} | all-to-all | bytes 2097152 | tf_op jit(solution)/shard_map/all_to_all | solution.py:140
  84.9 1.6 copy.100
  86.8 1.8 fusion.20
  88.6 1.5 div.38
  90.1 2.5 reshape.280
  92.6 2.6 reshape.281
  95.2 1.4 reshape.275
  96.7 1.4 fusion.22
  98.1 4.2 %multiply_convert_fusion.2 = (bf16[16,64,2,128]{3,0,1,2:T(8,128)(2,1)}, bf16[16,64,2,128]{3,0,1,2:T(8,128)(2,1)S(1)}, bf16[16,64,2,128]{3,0,1,2:T(8,128)(2,1)}) fusion(f32[16,64,2,128]{3,0,1,2:T(8,128)S(1)} %fusion.22, f32[16,64,2,128]{3,2,1,0:T(2,128)} %reshape.281, f32[16,2,128]{2,0,1:T(8,128)S(1)} %slice_bitcast_fusion.4, f32[16,64,2,128]{3,2,1,0:T(2,128)} %reshape.280), kind=kLoop, calls=%fused_computation.40 | loop fusion | flops 2097152 | bytes 4734976 | tf_op jit(solution)/shard_map/convert_element_type | solution.py:65
  102.3 2.7 fusion.24
  105.0 30.8 %all-gather.8.cloned.1.call-done = bf16[8,32,4,4096]{3,1,2,0:T(8,128)(2,1)} async-done(((bf16[1,32,4,4096]{3,1,2,0:T(8,128)(2,1)}), bf16[8,32,4,4096]{3,1,2,0:T(8,128)(2,1)}) %all-gather.8.cloned.1.call-update) | async-done | bytes 8388624 | tf_op jit(solution)/shard_map/all_gather | solution.py:139
  135.8 6.5 %fusion.8 = f32[8,32,4,256]{3,1,2,0:T(8,128)S(1)} fusion(bf16[8,32,4,4096]{3,1,2,0:T(8,128)(2,1)} %all-gather.8.cloned.1.call-done, bf16[1,4096,256]{2,1,0:T(8,128)(2,1)} %param.24), kind=kOutput, calls=%fused_computation.21 | convolution fusion | flops 2147483648 | bytes 11534336 | tf_op jit(solution)/shard_map/pskd,df->pskf/dot_general | solution.py:145
  142.7 2.4 fusion.15
  145.1 5.6 %convolution_convert_fusion = bf16[8,32,4,4096]{3,1,2,0:T(8,128)(2,1)} fusion(bf16[8,32,4,256]{3,1,2,0:T(8,128)(2,1)S(1)} %fusion.15, bf16[1,256,4096]{2,1,0:T(8,128)(2,1)S(1)} %copy-done), kind=kOutput, calls=%fused_computation.9 | convolution fusion | flops 2151677952 | bytes 11010048 | tf_op jit(solution)/shard_map/pskf,fd->pskd/dot_general | solution.py:149
  150.8 29.7 %while.17 = (s32[]{:T(128)}, f32[2,128,256]{2,1,0:T(8,128)S(1)}, f32[2,128]{1,0:T(2,128)S(1)}, f32[16,2,128,256]{3,2,1,0:T(8,128)}, f32[16,2,128]{2,1,0:T(2,128)...) while((s32[]{:T(128)}, f32[2,128,256]{2,1,0:T(8,128)S(1)}, ...), condition=%wide.region_2.3_spmd.clone, body=%wide.region_1.2_spmd.clone.sunk | while | flops 262915 | bytes 1319542 | solution.py:82
  151.5 1.1 bitcast_add_fusion.4
  152.6 0.7 bitcast_dynamic-update-slice_fusion.4
  153.4 1.1 bitcast_add_fusion.4
  154.5 0.7 bitcast_dynamic-update-slice_fusion.4
  155.2 1.1 bitcast_add_fusion.4
  157.1 1.1 bitcast_add_fusion.4
  158.9 1.1 bitcast_add_fusion.4
  160.8 1.1 bitcast_add_fusion.4
  162.6 1.1 bitcast_add_fusion.4
  164.5 1.1 bitcast_add_fusion.4
  166.4 1.1 bitcast_add_fusion.4
  167.5 0.7 bitcast_dynamic-update-slice_fusion.4
  168.2 1.1 bitcast_add_fusion.4
  169.4 0.7 bitcast_dynamic-update-slice_fusion.4
  170.1 1.1 bitcast_add_fusion.4
  171.9 1.1 bitcast_add_fusion.4
  173.8 1.1 bitcast_add_fusion.4
  174.9 0.7 bitcast_dynamic-update-slice_fusion.4
  175.7 1.1 bitcast_add_fusion.4
  177.5 1.1 bitcast_add_fusion.4
  178.7 0.7 bitcast_dynamic-update-slice_fusion.4
  179.4 1.1 bitcast_add_fusion.4
  180.6 7.8 %all-gather.2 = bf16[4,2,128]{2,1,0:T(2,128)(2,1)S(1)} all-gather(bf16[1,2,128]{2,1,0:T(2,128)(2,1)S(1)} %convert_bitcast_fusion.1), channel_id=2, replica_groups=mesh['ep_0'=8,'ep_1'=4,'tp'=8] {'ep_1'}, dimensions={0}, use_global_device_ids=true | all-gather | bytes 2560 | tf_op jit(solution)/shard_map/all_gather | solution.py:26
  188.4 12.2 %all-gather.1 = bf16[8,128,256]{2,1,0:T(8,128)(2,1)S(1)} all-gather(bf16[2,128,256]{2,1,0:T(8,128)(2,1)S(1)} %convert_element_type.277), channel_id=3, replica_groups=mesh['ep_0'=8,'ep_1'=4,'tp'=8] {'ep_1'}, dimensions={0}, use_global_device_ids=true | all-gather | bytes 655360 | tf_op jit(solution)/shard_map/all_gather | solution.py:26
  200.6 0.8 copy-done.1
  201.4 0.9 fusion.44
  202.6 3.5 %reduce-scatter.2.cloned.1.call-done = bf16[1,32,4,4096]{3,1,2,0:T(8,128)(2,1)} async-done(((bf16[8,32,4,4096]{3,1,2,0:T(8,128)(2,1)}), bf16[1,32,4,4096]{3,1,2,0:T(8,128)(2,1)}) %reduce-scatter.2.cloned.1.call-update) | async-done | bytes 1048592 | tf_op jit(solution)/shard_map/reduce_scatter | solution.py:148
  206.1 3.0 %copy.101 = bf16[1,32,4,4096]{3,2,0,1:T(4,128)(2,1)} copy(bf16[1,32,4,4096]{3,1,2,0:T(8,128)(2,1)} %reduce-scatter.2.cloned.1.call-done) | data formatting | bytes 2097152 | tf_op jit(solution)/shard_map/reduce_scatter | solution.py:148
  209.1 10.2 %all-to-all-start.1 = ((bf16[1,32,4,4096]{3,2,0,1:T(4,128)(2,1)}), bf16[1,32,4,4096]{3,2,0,1:T(4,128)(2,1)}, u32[]{:S(2)}, u32[]{:S(2)}) async-start(bf16[1,32,4,4096]{3,2,0,1:T(4,128)(2,1)} %copy.101), calls=%async_computation.2 | async-start | bytes 2097152 | tf_op jit(solution)/shard_map/all_to_all | solution.py:156
  219.5 41.7 %all_gather.25 = bf16[8,2,128]{2,1,0:T(2,128)(2,1)S(1)} all-gather(bf16[1,2,128]{2,1,0:T(2,128)(2,1)S(1)} %get-tuple-element.129), channel_id=1, replica_groups=mesh['ep_0'=8,'ep_1'=4,'tp'=8] {'ep_0'}, dimensions={0}, use_global_device_ids=true | all-gather | bytes 4608 | tf_op jit(solution)/shard_map/all_gather | solution.py:26
  261.2 2.0 fusion.42
  263.2 4.7 %fusion.4 = f32[16,2,256,64]{2,3,1,0:T(8,128)} fusion(f32[16,2,128,256]{3,2,1,0:T(8,128)} %get-tuple-element.42, f32[16,2,128]{2,1,0:T(2,128)S(1)} %get-tuple-element.45, f32[2,128,256]{2,1,0:T(8,128)S(1)} %fusion.42, bf16[16,64,2,128]{3,0,1,2:T(8,128)(2,1)} %get-tuple-element.121), kind=kOutput, calls=%fused_computation.17 | convolution fusion | flops 137363456 | bytes 7094272 | tf_op jit(solution)/shard_map/nihd,nhde->nihe/dot_general | solution.py:98
  267.9 4.0 %multiply_reduce_fusion = (f32[16,64,2]{1,2,0:T(2,128)S(1)}, f32[16,64,2,256]{3,1,2,0:T(8,128)}) fusion(f32[16,2,256,64]{2,3,1,0:T(8,128)} %fusion.4, bf16[16,64,2,256]{3,2,1,0:T(2,128)(2,1)S(1)} %reshape.275, bf16[16,64,2,128]{3,0,1,2:T(8,128)(2,1)} %get-tuple-element.119, pred[64,64]{1,0:T(8,128)(4,1)S(1)} %iota_compare_fusion.3, ...), kind=kOutput, calls=%fused_computation.25 | convolution fusion | flops 102496256 | bytes 6303744 | tf_op jit(solution)/shard_map/nhij,njhe->nihe/dot_general | solution.py:96
  271.9 1.9 multiply_convert_fusion
  273.9 1.1 copy.93
  275.0 1.2 copy.108
  276.2 1.3 reshape.278
  277.5 1.7 gather_fusion.1
  279.2 1.7 reshape.336
  280.9 1.4 multiply_reduce_fusion.1
  282.5 0.8 multiply_convert_fusion.3
  (123 shorter events, 10.9 us)
Async XLA Ops:
  8.0 137.1 %copy-start = (bf16[1,256,4096]{2,1,0:T(8,128)(2,1)S(1)}, bf16[1,256,4096]{2,1,0:T(8,128)(2,1)}, u32[]{:S(2)}) copy-start(bf16[1,256,4096]{2,1,0:T(8,128)(2,1)} %param.26) | copy-start | bytes 6291460
  8.0 127.8 %all-gather.8.cloned.1.call-start = ((), (), s32[]{:S(2)}) async-start(), calls=%async_computation.4 | async-start | bytes 9437184 | tf_op jit(solution)/shard_map/all_gather | solution.py:139
  11.9 24.2 %copy-start.2 = (f32[4096]{0:T(1024)S(1)}, f32[4096]{0:T(1024)}, u32[]{:S(2)}) copy-start(f32[4096]{0:T(1024)} %param.21) | copy-start | bytes 49156
  86.5 119.6 %reduce-scatter.2.cloned.1.call-start = ((), (), s32[]{:S(2)}) async-start(), calls=%async_computation.5 | async-start | bytes 9437184 | tf_op jit(solution)/shard_map/reduce_scatter | solution.py:148
  135.8 6.5 %copy-start.6 = (bf16[8,32,4,4096]{3,1,2,0:T(8,128)(2,1)S(1)}, bf16[8,32,4,4096]{3,1,2,0:T(8,128)(2,1)}, u32[]{:S(2)}) copy-start(bf16[8,32,4,4096]{3,1,2,0:T(8,128)(2,1)} %all-gather.8.cloned.1.call-done) | copy-start | bytes 25165828
  135.8 7.0 %copy-start.7 = (bf16[1,4096,256]{2,1,0:T(8,128)(2,1)S(1)}, bf16[1,4096,256]{2,1,0:T(8,128)(2,1)}, u32[]{:S(2)}) copy-start(bf16[1,4096,256]{2,1,0:T(8,128)(2,1)} %param.25) | copy-start | bytes 6291460
  150.7 110.5 %all-gather.6.cloned.1.call-start = ((), (), s32[]{:S(2)}) async-start(), calls=%async_computation.3 | async-start | bytes 1179648 | tf_op jit(solution)/shard_map/all_gather | solution.py:26
  180.5 38.8 %copy-start.5 = (f32[256,2]{0,1:T(2,128)S(1)}, f32[256,2]{0,1:T(2,128)}, u32[]{:S(2)}) copy-start(f32[256,2]{0,1:T(2,128)} %param.23) | copy-start | bytes 6148
  200.6 0.8 copy-start.1
  209.1 67.0 %all-to-all-start.1 = ((bf16[1,32,4,4096]{3,2,0,1:T(4,128)(2,1)}), bf16[1,32,4,4096]{3,2,0,1:T(4,128)(2,1)}, u32[]{:S(2)}, u32[]{:S(2)}) async-start(bf16[1,32,4,4096]{3,2,0,1:T(4,128)(2,1)} %copy.101), calls=%async_computation.2 | async-start | bytes 2097152 | tf_op jit(solution)/shard_map/all_to_all | solution.py:156
  267.9 4.0 %copy-start.4 = (f32[256]{0:T(256)S(1)}, f32[256]{0:T(256)}, u32[]{:S(2)}) copy-start(f32[256]{0:T(256)} %param.19) | copy-start | bytes 3076
  277.5 5.0 %copy-start.3 = (f32[4096]{0:T(1024)S(1)}, f32[4096]{0:T(1024)}, u32[]{:S(2)}) copy-start(f32[4096]{0:T(1024)} %param.27) | copy-start | bytes 49156
Sparse Core Ops, SparseCore 0:
  86.6 49.1 all-gather.7
  150.8 55.2 reduce-scatter.1
Sparse Core Ops, SparseCore 1:
  202.3 48.2 all-gather.5
where the time goes:
time: 292 us; the launch traced here: 291 us
  blocking collectives  101 us (35%)
  local copies, waits for them, and re-layouts  52.2 us (18%)
  other arithmetic  50.2 us (17%)
  waiting for transfers between devices  34.3 us (12%)
  matrix products  25.8 us (9%)
  between operations  15.9 us (5%)
  starting transfers between devices  10.5 us (4%)
    all_gather x3, blocking collectives, prefix_by_axis(): lax.all_gather(part.astype(kind), axis)  61.7 us
    all_to_all x1, blocking collectives, routed_experts(): lax.all_to_all(outgoing, EP, split_axis=1, concat_axis=1, tiled=True)  39.7 us
    all_gather x1, waiting for transfers between devices, routed_experts(): lax.all_gather(lax.all_to_all(outgoing, EP, split_axis=1, concat_axis=1,...  30.8 us
    scatter x1, local copies, waits for them, and re-layouts, routed_experts(): table = jnp.full((tp_count, experts * capacity), ep_rows, jnp.int32).at[s...  22.1 us
    add x16, other arithmetic, advance(): carry_state * block_decay[..., None] + block_update  17.1 us
    dynamic_update_slice x32, other arithmetic, token_mixer(): lax.scan(advance, start_carry, (update, step_decay))  11.8 us
    all_to_all x1, starting transfers between devices, routed_experts(): lax.all_to_all(summed, EP, split_axis=1, concat_axis=1, tiled=True)  10.2 us
    dot_general x1, matrix products, routed_experts(): jnp.einsum('pskd,df->pskf', arrived, gate_local, preferred_element_type=j...  6.46 us
  transfers between devices with their start and end apart: 4, of which 2 were waited for; matrix products, arithmetic and copies ran while one was open for 23% of the time, Pallas kernels for 0%

commit v1 on v0

--- a/solution.py
+++ b/solution.py
@@ -136,11 +136,17 @@
     down_local = down_weight[0]
     own_table = lax.dynamic_slice_in_dim(table, part_index, 1, 0)
     outgoing = padded[own_table].reshape(1, ep_count, capacity, model_width)
-    arrived = lax.all_gather(
-        lax.all_to_all(outgoing, EP, split_axis=1, concat_axis=1, tiled=True),
-        "tp",
+    arrived = jnp.concatenate(
+        lax.all_to_all(
+            jnp.stack(
+                [lax.all_to_all(outgoing, EP, split_axis=1, concat_axis=1, tiled=True)]
+                * lax.axis_size("tp")
+            ),
+            "tp",
+            0,
+            0,
+        ),
         axis=0,
-        tiled=True,
     )
     gate_act = jnp.einsum("pskd,df->pskf", arrived, gate_local, preferred_element_type=jnp.float32)
     up_act = jnp.einsum("pskd,df->pskf", arrived, up_local, preferred_element_type=jnp.float32)

time: 292 us -> 343 us (1.17)
  waiting for transfers between devices: 34.3 us -> 74.2 us
  local copies, waits for them, and re-layouts: 52.2 us -> 56 us
    all_to_all x0 -> x1, waiting for transfers between devices: none -> 74.1 us  [routed_experts(): lax.all_to_all(jnp.stack([lax.all_to_all(outgoing, EP, split_axis=1, conc...]
    all_gather x1 -> x0, waiting for transfers between devices: 30.8 us -> none  [routed_experts(): lax.all_gather(lax.all_to_all(outgoing, EP, split_axis=1, concat_axis=1,...]
    all_to_all x0 -> x1, starting transfers between devices: none -> 4.96 us  [routed_experts(): lax.all_to_all(jnp.stack([lax.all_to_all(outgoing, EP, split_axis=1, conc...]
    another operation x0 -> x1, local copies, waits for them, and re-layouts: none -> 4.26 us  [routed_experts(): jnp.stack([lax.all_to_all(outgoing, EP, split_axis=1, concat_axis=1, tile...]
    reduce_scatter x1, waiting for transfers between devices: 3.47 us -> 0.02 us  [routed_experts(): lax.psum_scatter(jnp.einsum('pskf,fd->pskd', hidden, down_local, preferre...]
  transfers between devices with their start and end apart: 4 -> 4, of which waited for: 2 -> 1; matrix products, arithmetic and copies ran while one was open for 23% -> 20% of each run, Pallas kernels for 0% -> 0%
where the time goes in v1:
time: 343 us; the launch traced here: 342 us
  blocking collectives  101 us (29%)
  waiting for transfers between devices  74.2 us (22%)
  local copies, waits for them, and re-layouts  56 us (16%)
  other arithmetic  51.3 us (15%)
  matrix products  29.2 us (9%)
  between operations  15.9 us (5%)
  starting transfers between devices  13.3 us (4%)
    all_to_all x1, waiting for transfers between devices, routed_experts(): lax.all_to_all(jnp.stack([lax.all_to_all(outgoing, EP, split_axis=1, conc...  74.1 us
    all_gather x3, blocking collectives, prefix_by_axis(): lax.all_gather(part.astype(kind), axis)  61.6 us
    all_to_all x1, blocking collectives, routed_experts(): lax.all_to_all(outgoing, EP, split_axis=1, concat_axis=1, tiled=True)  39.7 us
    scatter x1, local copies, waits for them, and re-layouts, routed_experts(): table = jnp.full((tp_count, experts * capacity), ep_rows, jnp.int32).at[s...  22.1 us
    add x16, other arithmetic, advance(): carry_state * block_decay[..., None] + block_update  17.1 us
    dynamic_update_slice x32, other arithmetic, token_mixer(): lax.scan(advance, start_carry, (update, step_decay))  11.9 us
    all_to_all x1, starting transfers between devices, routed_experts(): lax.all_to_all(summed, EP, split_axis=1, concat_axis=1, tiled=True)  8.08 us
  transfers between devices with their start and end apart: 4, of which 1 were waited for; matrix products, arithmetic and copies ran while one was open for 20% of the time, Pallas kernels for 0%

profile of v1, /device:TPU:2, one launch (start us, length us, event | category | flops | bytes accessed | tf_op | source)
XLA Modules:
  0.0 341.8 jit_solution(10895617428590153386)
XLA Ops:
  8.0 0.8 broadcast_multiply_fusion
  8.9 0.8 copy.96
  9.7 2.1 fusion.5
  12.5 1.3 fusion.79
  14.0 22.1 %scatter_fusion = s32[8,128]{1,0:T(8,128)S(1)} fusion(s32[8,128]{1,0:T(8,128)S(1)} %broadcast_in_dim.33, s32[512]{0:T(512)S(1)} %reshape.316, s32[512]{0:T(512)S(1)} %reshape.318), kind=kCustom, calls=%fused_computation.2 | custom fusion | bytes 10240 | tf_op jit(solution)/shard_map/scatter | solution.py:132
  36.1 2.2 fusion.7
  38.3 1.5 concatenate.6
  39.9 4.1 %gather_fusion = bf16[128,4096]{1,0:T(8,128)(2,1)S(1)} fusion(bf16[257,4096]{1,0:T(8,128)(2,1)} %concatenate.6, s32[1024]{0:T(1024)S(1)} %pad_clamp_fusion.1), kind=kCustom, calls=%fused_computation | custom fusion | bytes 2097664 | tf_op jit(solution)/shard_map/gather | solution.py:138
  44.0 1.2 reshape.283
  45.2 39.7 %all_to_all.18 = bf16[1,32,4,4096]{3,2,0,1:T(4,128)(2,1)S(1)} all-to-all(bf16[1,32,4,4096]{3,2,0,1:T(4,128)(2,1)} %bitcast.187), channel_id=1, replica_groups=mesh['ep_0'=8,'ep_1'=4,'tp'=8] {'ep_0','ep_1'}, dimensions={1} | all-to-all | bytes 2097152 | tf_op jit(solution)/shard_map/all_to_all | solution.py:142
  85.5 4.3 %stack.2 = bf16[8,1,32,4,4096]{4,2,3,1,0:T(8,128)(2,1)} broadcast(bf16[32,4,4096]{2,0,1:T(8,128)(2,1)S(1)} %copy.101), dimensions={2,3,4} | broadcast | bytes 9437184 | tf_op jit(solution)/shard_map/stack | solution.py:141
  89.7 5.0 %all-to-all-start.1 = ((bf16[8,1,32,4,4096]{4,2,3,1,0:T(8,128)(2,1)}), bf16[8,1,32,4,4096]{4,2,3,1,0:T(8,128)(2,1)}, u32[]{:S(2)}, u32[]{:S(2)}) async-start(bf16[8,1,32,4,4096]{4,2,3,1,0:T(8,128)(2,1)} %stack.2), calls=%async_computation.1 | async-start | bytes 16777216 | tf_op jit(solution)/shard_map/all_to_all | solution.py:140
  95.0 1.3 reshape.281
  96.3 2.6 reshape.287
  98.9 2.5 reshape.288
  101.4 2.8 fusion.26
  104.2 2.7 div.38
  107.0 1.3 fusion.28
  108.3 4.1 %multiply_convert_fusion.2 = (bf16[16,64,2,128]{3,0,1,2:T(8,128)(2,1)}, bf16[16,64,2,128]{3,0,1,2:T(8,128)(2,1)S(1)}, bf16[16,64,2,128]{3,0,1,2:T(8,128)(2,1)}) fusion(f32[16,64,2,128]{3,0,1,2:T(8,128)S(1)} %fusion.28, f32[16,64,2,128]{3,2,1,0:T(2,128)} %reshape.288, f32[16,2,128]{2,0,1:T(8,128)S(1)} %slice_bitcast_fusion.4, f32[16,64,2,128]{3,2,1,0:T(2,128)} %reshape.287), kind=kLoop, calls=%fused_computation.42 | loop fusion | flops 2097152 | bytes 4734976 | tf_op jit(solution)/shard_map/convert_element_type | solution.py:65
  112.4 2.7 fusion.30
  115.1 74.1 %all-to-all-done.1 = bf16[8,1,32,4,4096]{4,2,3,1,0:T(8,128)(2,1)} async-done(((bf16[8,1,32,4,4096]{4,2,3,1,0:T(8,128)(2,1)}), bf16[8,1,32,4,4096]{4,2,3,1,0:T(8,128)(2,1)}, u32[]{:S(2)}, u32[]{:S(2)}) %all-to-all-start.1) | async-done | bytes 8388640 | tf_op jit(solution)/shard_map/all_to_all | solution.py:140
  189.3 6.5 %fusion.3 = f32[8,32,4,256]{3,1,2,0:T(8,128)S(1)} fusion(bf16[8,1,32,4,4096]{4,2,3,1,0:T(8,128)(2,1)} %all-to-all-done.1, bf16[1,4096,256]{2,1,0:T(8,128)(2,1)} %param.24), kind=kOutput, calls=%fused_computation.11 | convolution fusion | flops 2147483648 | bytes 11534336 | tf_op jit(solution)/shard_map/pskd,df->pskf/dot_general | solution.py:151
  195.8 5.8 %fusion.19 = bf16[8,32,4,256]{3,1,2,0:T(8,128)(2,1)S(1)} fusion(bf16[1,4096,256]{2,1,0:T(8,128)(2,1)S(1)} %copy-done.6, bf16[8,1,32,4,4096]{4,2,3,1,0:T(8,128)(2,1)} %all-to-all-done.1, f32[8,32,4,256]{3,1,2,0:T(8,128)S(1)} %fusion.3), kind=kOutput, calls=%fused_computation.32 | convolution fusion | flops 2149056512 | bytes 12058624 | tf_op jit(solution)/shard_map/pskd,df->pskf/dot_general | solution.py:152
  201.5 5.6 %convolution_convert_fusion = bf16[8,32,4,4096]{3,1,2,0:T(8,128)(2,1)} fusion(bf16[8,32,4,256]{3,1,2,0:T(8,128)(2,1)S(1)} %fusion.19, bf16[1,256,4096]{2,1,0:T(8,128)(2,1)S(1)} %copy-done), kind=kOutput, calls=%fused_computation.13 | convolution fusion | flops 2151677952 | bytes 11010048 | tf_op jit(solution)/shard_map/pskf,fd->pskd/dot_general | solution.py:155
  207.2 30.0 %while.17 = (s32[]{:T(128)}, f32[2,128,256]{2,1,0:T(8,128)S(1)}, f32[2,128]{1,0:T(2,128)S(1)}, f32[16,2,128,256]{3,2,1,0:T(8,128)}, f32[16,2,128]{2,1,0:T(2,128)...) while((s32[]{:T(128)}, f32[2,128,256]{2,1,0:T(8,128)S(1)}, ...), condition=%wide.region_2.3_spmd.clone, body=%wide.region_1.2_spmd.clone.sunk | while | flops 262915 | bytes 1319042 | solution.py:82
  208.0 1.1 bitcast_add_fusion.4
  209.8 1.1 bitcast_add_fusion.4
  211.7 1.1 bitcast_add_fusion.4
  213.6 1.1 bitcast_add_fusion.4
  214.7 0.7 bitcast_dynamic-update-slice_fusion.4
  215.5 1.1 bitcast_add_fusion.4
  216.6 0.7 bitcast_dynamic-update-slice_fusion.4
  217.4 1.1 bitcast_add_fusion.4
  219.2 1.1 bitcast_add_fusion.4
  221.1 1.1 bitcast_add_fusion.4
  222.3 0.7 bitcast_dynamic-update-slice_fusion.4
  223.0 1.1 bitcast_add_fusion.4
  224.9 1.1 bitcast_add_fusion.4
  226.7 1.1 bitcast_add_fusion.4
  227.9 0.7 bitcast_dynamic-update-slice_fusion.4
  228.6 1.1 bitcast_add_fusion.4
  229.8 0.7 bitcast_dynamic-update-slice_fusion.4
  230.5 1.1 bitcast_add_fusion.4
  232.4 1.1 bitcast_add_fusion.4
  234.2 1.1 bitcast_add_fusion.4
  236.1 1.1 bitcast_add_fusion.4
  237.2 7.8 %all-gather.2 = bf16[4,2,128]{2,1,0:T(2,128)(2,1)S(1)} all-gather(bf16[1,2,128]{2,1,0:T(2,128)(2,1)S(1)} %convert_bitcast_fusion.1), channel_id=2, replica_groups=mesh['ep_0'=8,'ep_1'=4,'tp'=8] {'ep_1'}, dimensions={0}, use_global_device_ids=true | all-gather | bytes 2560 | tf_op jit(solution)/shard_map/all_gather | solution.py:26
  245.1 12.2 %all-gather.1 = bf16[8,128,256]{2,1,0:T(8,128)(2,1)S(1)} all-gather(bf16[2,128,256]{2,1,0:T(8,128)(2,1)S(1)} %convert_element_type.277), channel_id=3, replica_groups=mesh['ep_0'=8,'ep_1'=4,'tp'=8] {'ep_1'}, dimensions={0}, use_global_device_ids=true | all-gather | bytes 655360 | tf_op jit(solution)/shard_map/all_gather | solution.py:26
  257.3 0.8 copy-done.1
  258.0 0.9 fusion.50
  259.3 3.0 copy.102
  262.3 8.1 %all-to-all-start.2 = ((bf16[1,32,4,4096]{3,2,0,1:T(4,128)(2,1)}), bf16[1,32,4,4096]{3,2,0,1:T(4,128)(2,1)}, u32[]{:S(2)}, u32[]{:S(2)}) async-start(bf16[1,32,4,4096]{3,2,0,1:T(4,128)(2,1)} %copy.102), calls=%async_computation.3 | async-start | bytes 2097152 | tf_op jit(solution)/shard_map/all_to_all | solution.py:162
  270.6 41.6 %all_gather.22 = bf16[8,2,128]{2,1,0:T(2,128)(2,1)S(1)} all-gather(bf16[1,2,128]{2,1,0:T(2,128)(2,1)S(1)} %get-tuple-element.129), channel_id=1, replica_groups=mesh['ep_0'=8,'ep_1'=4,'tp'=8] {'ep_0'}, dimensions={0}, use_global_device_ids=true | all-gather | bytes 4608 | tf_op jit(solution)/shard_map/all_gather | solution.py:26
  312.2 2.0 fusion.48
  314.2 4.7 %fusion.8 = f32[16,2,256,64]{2,3,1,0:T(8,128)} fusion(f32[16,2,128,256]{3,2,1,0:T(8,128)} %get-tuple-element.42, f32[16,2,128]{2,1,0:T(2,128)S(1)} %get-tuple-element.45, f32[2,128,256]{2,1,0:T(8,128)S(1)} %fusion.48, bf16[16,64,2,128]{3,0,1,2:T(8,128)(2,1)} %get-tuple-element.121), kind=kOutput, calls=%fused_computation.21 | convolution fusion | flops 137363456 | bytes 7094272 | tf_op jit(solution)/shard_map/nihd,nhde->nihe/dot_general | solution.py:98
  318.9 4.0 %multiply_reduce_fusion = (f32[16,64,2]{1,2,0:T(2,128)S(1)}, f32[16,64,2,256]{3,1,2,0:T(8,128)}) fusion(f32[16,2,256,64]{2,3,1,0:T(8,128)} %fusion.8, bf16[16,64,2,256]{3,2,1,0:T(2,128)(2,1)S(1)} %reshape.281, bf16[16,64,2,128]{3,0,1,2:T(8,128)(2,1)} %get-tuple-element.119, pred[64,64]{1,0:T(8,128)(4,1)S(1)} %iota_compare_fusion.3, ...), kind=kOutput, calls=%fused_computation.27 | convolution fusion | flops 102496256 | bytes 6303744 | tf_op jit(solution)/shard_map/nhij,njhe->nihe/dot_general | solution.py:96
  322.9 1.9 multiply_convert_fusion
  324.9 1.1 copy.94
  326.0 1.2 copy.109
  327.2 1.3 reshape.285
  328.5 1.7 gather_fusion.1
  330.2 1.7 reshape.343
  331.9 1.4 multiply_reduce_fusion.1
  333.5 0.8 multiply_convert_fusion.3
  (121 shorter events, 11.2 us)
Async XLA Ops:
  8.0 193.5 %copy-start = (bf16[1,256,4096]{2,1,0:T(8,128)(2,1)S(1)}, bf16[1,256,4096]{2,1,0:T(8,128)(2,1)}, u32[]{:S(2)}) copy-start(bf16[1,256,4096]{2,1,0:T(8,128)(2,1)} %param.26) | copy-start | bytes 6291460
  14.0 22.1 %copy-start.2 = (f32[4096]{0:T(1024)S(1)}, f32[4096]{0:T(1024)}, u32[]{:S(2)}) copy-start(f32[4096]{0:T(1024)} %param.21) | copy-start | bytes 49156
  89.7 99.6 %all-to-all-start.1 = ((bf16[8,1,32,4,4096]{4,2,3,1,0:T(8,128)(2,1)}), bf16[8,1,32,4,4096]{4,2,3,1,0:T(8,128)(2,1)}, u32[]{:S(2)}, u32[]{:S(2)}) async-start(bf16[8,1,32,4,4096]{4,2,3,1,0:T(8,128)(2,1)} %stack.2), calls=%async_computation.1 | async-start | bytes 16777216 | tf_op jit(solution)/shard_map/all_to_all | solution.py:140
  94.7 164.6 %reduce-scatter.2.cloned.1.call-start = ((), (), s32[]{:S(2)}) async-start(), calls=%async_computation.5 | async-start | bytes 9437184 | tf_op jit(solution)/shard_map/reduce_scatter | solution.py:154
  189.3 6.5 %copy-start.6 = (bf16[1,4096,256]{2,1,0:T(8,128)(2,1)S(1)}, bf16[1,4096,256]{2,1,0:T(8,128)(2,1)}, u32[]{:S(2)}) copy-start(bf16[1,4096,256]{2,1,0:T(8,128)(2,1)} %param.25) | copy-start | bytes 6291460
  207.1 105.1 %all-gather.5.cloned.1.call-start = ((), (), s32[]{:S(2)}) async-start(), calls=%async_computation.4 | async-start | bytes 1179648 | tf_op jit(solution)/shard_map/all_gather | solution.py:26
  237.2 33.2 %copy-start.5 = (f32[256,2]{0,1:T(2,128)S(1)}, f32[256,2]{0,1:T(2,128)}, u32[]{:S(2)}) copy-start(f32[256,2]{0,1:T(2,128)} %param.23) | copy-start | bytes 6148
  257.2 0.8 copy-start.1
  262.3 64.8 %all-to-all-start.2 = ((bf16[1,32,4,4096]{3,2,0,1:T(4,128)(2,1)}), bf16[1,32,4,4096]{3,2,0,1:T(4,128)(2,1)}, u32[]{:S(2)}, u32[]{:S(2)}) async-start(bf16[1,32,4,4096]{3,2,0,1:T(4,128)(2,1)} %copy.102), calls=%async_computation.3 | async-start | bytes 2097152 | tf_op jit(solution)/shard_map/all_to_all | solution.py:162
  318.9 4.0 %copy-start.4 = (f32[256]{0:T(256)S(1)}, f32[256]{0:T(256)}, u32[]{:S(2)}) copy-start(f32[256]{0:T(256)} %param.19) | copy-start | bytes 3076
  328.5 5.0 %copy-start.3 = (f32[4096]{0:T(1024)S(1)}, f32[4096]{0:T(1024)}, u32[]{:S(2)}) copy-start(f32[4096]{0:T(1024)} %param.27) | copy-start | bytes 49156
Sparse Core Ops, SparseCore 0:
  207.2 49.8 reduce-scatter.1
Sparse Core Ops, SparseCore 1:
  259.0 43.1 all-gather.4
